TPU v7x, 32 devices: a whole 2x2x4 slice. The times are simulated.
32 devices in a mesh: grp: 2 (over y), sp: 4 (over z), tp: 4 (over x, core).
Axes of the slice: x: 2, y: 2, z: 4, core: 2. Of those that a mesh axis runs over, the one named last changes fastest.
Arguments:
- tokens: bfloat16 [1024, 2048], P(('grp', 'sp')), parts along dimension 0, may hold values from -8 to 8
- norm_gain: float32 [2048], replicated, may hold values from 0.1 to 1.9
- w_query: bfloat16 [2048, 1024], P(None, 'tp'), may hold values from -0.125 to 0.125
- w_key: bfloat16 [2048, 1024], P(None, 'tp'), may hold values from -0.125 to 0.125
- w_value: bfloat16 [2048, 1024], P(None, 'tp'), may hold values from -0.125 to 0.125
- w_out: bfloat16 [1024, 2048], P('tp'), may hold values from -0.1875 to 0.1875
- key_rate: bfloat16 [16, 1024], P('tp', ('grp', 'sp')), parts along dimension 1, may hold values from -16 to 1
Outputs:
- layer_out: bfloat16 [1024, 2048], P(('grp', 'sp')), parts along dimension 0
There are 2 independent parts, one for each index of `grp`. A program takes and returns all parts, laid end to end along the dimension named above; an argument that names none is the same for every part. Nothing has to cross between parts.
All inputs are finite; a program needn't handle non-finite values.
Results may differ from a plain program's by a relative error of at most 0.0075.
Values may be sent and summed in bfloat16 or wider, within the bound.
No kernel may reach another device: no remote copies, remote signals or barrier semaphores. Data moves between devices by JAX's collectives and lax.ppermute only.
A program may use at most 64 MiB of HBM per device.

v0:
```python
import jax
import jax.numpy as jnp
from jax import lax
from jax.sharding import PartitionSpec as P

HD = 64
KEY_SPAN = 128
F32 = jnp.float32
BF16 = jnp.bfloat16
HIGHEST = lax.Precision.HIGHEST
EPS = 1e-06


def break_scores(query_heads, key_heads, rate_row_values, query_pos, key_pos):
    scores = jnp.einsum(
        "qhd,khd->hqk", query_heads, key_heads, preferred_element_type=F32
    ) * HD ** (-0.5)
    scores = scores + jnp.transpose(rate_row_values).astype(F32)[:, None, :]
    causal_mask = key_pos[None, :] < query_pos[:, None]
    log_remain = jnp.where(causal_mask[None], jax.nn.log_sigmoid(-scores), 0.0)
    return (scores, causal_mask, log_remain)


def shard_summary(query_heads, key_heads, value_heads, rate_row_values, query_pos, key_pos):
    scores, causal_mask, log_remain = break_scores(
        query_heads, key_heads, rate_row_values, query_pos, key_pos
    )
    heads_here, query_count, key_count = scores.shape
    span_count = key_count // KEY_SPAN
    blocks = log_remain.reshape(heads_here, query_count, span_count, KEY_SPAN)
    span_ids = jnp.arange(KEY_SPAN, dtype=jnp.int32)
    tri_strict = (span_ids[:, None] > span_ids[None, :]).astype(F32)
    inside_sum = jnp.einsum("hqnj,js->hqns", blocks, tri_strict, precision=HIGHEST)
    block_ids = jnp.arange(span_count, dtype=jnp.int32)
    block_later = (block_ids[:, None] > block_ids[None, :]).astype(F32)
    beyond = jnp.einsum("hqn,nm->hqm", jnp.sum(blocks, axis=-1), block_later, precision=HIGHEST)
    suffix = (inside_sum + beyond[..., None]).reshape(heads_here, query_count, key_count)
    weight = jnp.where(causal_mask[None], jnp.exp(jax.nn.log_sigmoid(scores) + suffix), 0.0).astype(
        BF16
    )
    partial_value = jnp.einsum("hqk,khd->qhd", weight, value_heads, preferred_element_type=F32)
    return (partial_value.reshape(query_count, heads_here * HD), jnp.sum(log_remain, axis=-1))


def on_device(tokens, norm_gain, w_query, w_key, w_value, w_out, key_rate):
    tokens_f = tokens.astype(F32)
    normed = (
        tokens_f
        * lax.rsqrt(jnp.mean(tokens_f * tokens_f, axis=-1, keepdims=True) + EPS)
        * norm_gain
    ).astype(BF16)
    queries = jnp.dot(normed, w_query, preferred_element_type=F32).astype(BF16)
    key_rows = jnp.dot(normed, w_key, preferred_element_type=F32).astype(BF16)
    value_rows = jnp.dot(normed, w_value, preferred_element_type=F32).astype(BF16)
    head_width = w_query.shape[1]
    heads_local = head_width // HD
    row_count = tokens.shape[0]
    rate_row_values = jnp.transpose(key_rate)
    query_heads = queries.reshape(row_count, heads_local, HD)
    own_shard = lax.axis_index("sp")
    shard_total = lax.axis_size("sp")
    local_pos = jnp.arange(row_count, dtype=jnp.int32)
    shard_ids = jnp.arange(shard_total, dtype=jnp.int32)
    later_mask = (shard_ids[:, None] > shard_ids[None, :]).astype(F32)
    query_groups = [(query_heads, own_shard * row_count)]

    def summarize(key_block, value_block, rate_block, first_key):
        key_pos = first_key + local_pos
        group_heads, group_start = query_groups[0]
        group_count = group_heads.shape[0]
        group_pos = group_start + jnp.arange(group_count, dtype=jnp.int32)
        empty_pair = (
            jnp.zeros((group_count, head_width), F32),
            jnp.zeros((heads_local, group_count), F32),
        )
        partial_value, remain = lax.cond(
            first_key < group_start + group_count - 1,
            lambda: shard_summary(
                group_heads, key_block, value_block, rate_block, group_pos, key_pos
            ),
            lambda: empty_pair,
        )
        partial_list = [partial_value]
        remain_list = [remain]
        return (jnp.concatenate(partial_list, axis=0), jnp.concatenate(remain_list, axis=1))

    initial = (
        jnp.zeros((shard_total, row_count, head_width), F32),
        jnp.zeros((shard_total, heads_local, row_count), F32),
    )
    piece_keys = lax.all_gather(key_rows, "sp", axis=0, tiled=True)
    piece_values = lax.all_gather(value_rows, "sp", axis=0, tiled=True)
    piece_rates = lax.all_gather(rate_row_values, "sp", axis=0, tiled=True)
    piece_count = piece_keys.shape[0] // row_count
    key_blocks = piece_keys.reshape(piece_count, row_count, heads_local, HD)
    value_blocks = piece_values.reshape(piece_count, row_count, heads_local, HD)
    rate_blocks = piece_rates.reshape(piece_count, row_count, heads_local)

    def absorb_one(inner_pair, item_tuple):
        item_index, key_block, value_block, rate_block = item_tuple
        first_key = item_index * row_count
        shard_index = first_key // row_count
        partial_value, remain = summarize(key_block, value_block, rate_block, first_key)
        partials = lax.dynamic_update_index_in_dim(inner_pair[0], partial_value, shard_index, 0)
        remains = lax.dynamic_update_index_in_dim(inner_pair[1], remain, shard_index, 0)
        return ((partials, remains), None)

    result, _ = lax.scan(
        absorb_one,
        initial,
        (jnp.arange(piece_count, dtype=jnp.int32), key_blocks, value_blocks, rate_blocks),
    )
    partials, remains = result
    beyond = jnp.einsum("nhq,nm->mhq", remains, later_mask, precision=HIGHEST)
    factor = jnp.transpose(jnp.exp(beyond), (0, 2, 1))[..., None]
    mixed_rows = jnp.sum(partials.reshape(shard_total, row_count, heads_local, HD) * factor, axis=0)
    mixed = mixed_rows.reshape(row_count, head_width).astype(BF16)
    token_heads = lax.all_to_all(mixed, "tp", split_axis=0, concat_axis=1, tiled=True)
    whole_out = lax.all_gather(w_out, "tp", axis=0, tiled=True)
    own_rows = jnp.dot(token_heads, whole_out, preferred_element_type=F32).astype(BF16)
    return lax.all_gather(own_rows, "tp", axis=0, tiled=True)


def solution(mesh):
    return jax.shard_map(
        on_device,
        mesh=mesh,
        in_specs=(
            P(("grp", "sp"), None),
            P(),
            P(None, "tp"),
            P(None, "tp"),
            P(None, "tp"),
            P("tp", None),
            P("tp", ("grp", "sp")),
        ),
        out_specs=P(("grp", "sp"), None),
        check_vma=False,
    )
```

profile of v0, /device:TPU:25, one launch (start us, length us, event | category | flops | bytes accessed | tf_op | source)
XLA Modules:
  0.0 93.3 jit_solution(17264272396755167459)
XLA Ops:
  6.5 0.7 all-gather.2.cloned.1.call-update
  7.3 1.2 %fusion.25 = f32[128]{0:T(128)S(1)} fusion(bf16[128,2048]{1,0:T(8,128)(2,1)} %param.11), kind=kLoop, calls=%fused_computation.40 | loop fusion | flops 786304 | bytes 524800 | tf_op jit(solution)/shard_map/reduce_sum | solution.py:49
  8.5 1.4 %convolution_convert_fusion.3 = bf16[128,256]{1,0:T(8,128)(2,1)S(1)} fusion(bf16[2048,256]{1,0:T(8,128)(2,1)S(1)} %copy-done, bf16[128,2048]{1,0:T(8,128)(2,1)} %param.11, f32[2048]{0:T(1024)} %param.12, f32[128]{0:T(128)S(1)} %add_rsqrt_fusion), kind=kOutput, calls=%fused_computation.37 | convolution fusion | flops 135299072 | bytes 1647104 | tf_op jit(solution)/shard_map/dot_general | solution.py:53
  9.9 11.0 %all_gather.15 = bf16[512,256]{1,0:T(8,128)(2,1)S(1)} all-gather(bf16[128,256]{1,0:T(8,128)(2,1)S(1)} %convolution_convert_fusion.3), channel_id=1, replica_groups=mesh['grp'=2,'sp'=4,'tp'=4] {'sp'}, dimensions={0}, use_global_device_ids=true | all-gather | bytes 327680 | tf_op jit(solution)/shard_map/all_gather | solution.py:91
  20.9 0.2 reshape.91
  21.2 0.3 copy.39
  21.5 1.6 %convolution_convert_fusion.1 = bf16[128,256]{1,0:T(8,128)(2,1)S(1)} fusion(bf16[2048,256]{1,0:T(8,128)(2,1)} %param.15, bf16[128,2048]{1,0:T(8,128)(2,1)S(1)} %copy-done.1, f32[2048]{0:T(1024)S(1)} %copy-done.3, f32[128]{0:T(128)S(1)} %add_rsqrt_fusion), kind=kOutput, calls=%fused_computation.35 | convolution fusion | flops 135299072 | bytes 1647104 | tf_op jit(solution)/shard_map/dot_general | solution.py:54
  23.1 12.0 %all_gather.17 = bf16[512,256]{1,0:T(8,128)(2,1)S(1)} all-gather(bf16[128,256]{1,0:T(8,128)(2,1)S(1)} %convolution_convert_fusion.1), channel_id=1, replica_groups=mesh['grp'=2,'sp'=4,'tp'=4] {'sp'}, dimensions={0}, use_global_device_ids=true | all-gather | bytes 327680 | tf_op jit(solution)/shard_map/all_gather | solution.py:92
  35.1 0.2 reshape.92
  35.3 0.3 copy.40
  35.6 1.6 %convolution_convert_fusion.2 = bf16[128,256]{1,0:T(8,128)(2,1)S(1)} fusion(bf16[2048,256]{1,0:T(8,128)(2,1)} %param.13, bf16[128,2048]{1,0:T(8,128)(2,1)S(1)} %copy-done.1, f32[2048]{0:T(1024)S(1)} %copy-done.3, f32[128]{0:T(128)S(1)} %add_rsqrt_fusion), kind=kOutput, calls=%fused_computation.36 | convolution fusion | flops 135299072 | bytes 1647104 | tf_op jit(solution)/shard_map/dot_general | solution.py:52
  37.2 0.1 copy.37
  37.3 5.6 %all_gather.16 = bf16[512,4]{0,1:T(4,128)(2,1)S(1)} all-gather(bf16[128,4]{0,1:T(4,128)(2,1)S(1)} %bitcast.58), channel_id=1, replica_groups=mesh['grp'=2,'sp'=4,'tp'=4] {'sp'}, dimensions={0}, use_global_device_ids=true | all-gather | bytes 5120 | tf_op jit(solution)/shard_map/all_gather | solution.py:93
  43.0 18.4 %while.16 = (s32[]{:T(128)}, f32[4,128,256]{1,2,0:T(8,128)S(1)}, f32[4,4,128]{2,0,1:T(4,128)S(1)}, s32[4]{0:T(128)S(1)}, s32[]{:T(128)}, /*index=5*/s32[]{:T(128...) while((s32[]{:T(128)}, f32[4,128,256]{1,2,0:T(8,128)S(1)}, ...), condition=%wide.region_5.6_spmd.clone, body=%wide.region_1.5_spmd.clone.sunk | while | flops 119505664 | bytes 1446895 | solution.py:108
  43.0 0.6 dynamic_slice.50
  44.3 2.6 %conditional.3 = (f32[1,128,256]{1,2,0:T(8,128)S(1)}, f32[1,4,128]{2,1,0:T(4,128)}) conditional(s32[]{:T(128)} %convert_element_type.82, () %tuple.61, (s32[]{:T(128)}, s32[128]{0:T(128)S(1)}, s32[]{:T(128)}, s32[128]{0:T(128)S(1)}, bf16[4,128,4,64]{1,3,2,0:T(8,128)(2,1)S(1)}, /*index=5*/s32[]{:T(128)}, bf16[128,4,64]{0,2,1:T(8,128)(2,1)S(1)}, ...), branch_computations={%region_2.2_spmd, %region_3.4_spmd} | conditional | flops 119505664 | bytes 1179684 | solution.py:76
  44.4 1.0 %fusion.11 = (f32[4,128]{1,0:T(4,128)}, f32[4,128,128]{1,2,0:T(8,128)S(1)}) fusion(pred[128,128]{0,1:T(8,128)(4,1)S(1)} %broadcast_compare_fusion, f32[4,128]{1,0:T(4,128)S(1)} %convert_bitcast_fusion, bf16[128,4,64]{0,2,1:T(8,128)(2,1)S(1)} %get-tuple-element.246, bf16[4,128,4,64]{1,3,2,0:T(8,128)(2,1)S(1)} %get-tuple-element.244, s32[]{:T(128)} %get-tuple-element.245), kind=kOutput, calls=%fused_computation.14 | convolution fusion | flops 9108992 | bytes 413700 | tf_op jit(solution)/shard_map/while/body/eval_jaxpr/cond/branch_1_fun/qhd,khd->hqk/dot_general | solution.py:15
  45.4 0.7 broadcast_multiply_fusion
  46.1 0.6 fusion.7
  46.7 0.2 fusion.14
  46.9 0.7 dynamic_update_slice.22
  47.6 0.6 dynamic_slice.50
  48.9 2.6 %conditional.3 = (f32[1,128,256]{1,2,0:T(8,128)S(1)}, f32[1,4,128]{2,1,0:T(4,128)}) conditional(s32[]{:T(128)} %convert_element_type.82, () %tuple.61, (s32[]{:T(128)}, s32[128]{0:T(128)S(1)}, s32[]{:T(128)}, s32[128]{0:T(128)S(1)}, bf16[4,128,4,64]{1,3,2,0:T(8,128)(2,1)S(1)}, /*index=5*/s32[]{:T(128)}, bf16[128,4,64]{0,2,1:T(8,128)(2,1)S(1)}, ...), branch_computations={%region_2.2_spmd, %region_3.4_spmd} | conditional | flops 119505664 | bytes 1179684 | solution.py:76
  49.0 1.0 %fusion.11 = (f32[4,128]{1,0:T(4,128)}, f32[4,128,128]{1,2,0:T(8,128)S(1)}) fusion(pred[128,128]{0,1:T(8,128)(4,1)S(1)} %broadcast_compare_fusion, f32[4,128]{1,0:T(4,128)S(1)} %convert_bitcast_fusion, bf16[128,4,64]{0,2,1:T(8,128)(2,1)S(1)} %get-tuple-element.246, bf16[4,128,4,64]{1,3,2,0:T(8,128)(2,1)S(1)} %get-tuple-element.244, s32[]{:T(128)} %get-tuple-element.245), kind=kOutput, calls=%fused_computation.14 | convolution fusion | flops 9108992 | bytes 413700 | tf_op jit(solution)/shard_map/while/body/eval_jaxpr/cond/branch_1_fun/qhd,khd->hqk/dot_general | solution.py:15
  50.0 0.7 broadcast_multiply_fusion
  50.7 0.6 fusion.7
  51.3 0.2 fusion.14
  51.5 0.7 dynamic_update_slice.22
  52.2 0.6 dynamic_slice.50
  53.5 2.6 %conditional.3 = (f32[1,128,256]{1,2,0:T(8,128)S(1)}, f32[1,4,128]{2,1,0:T(4,128)}) conditional(s32[]{:T(128)} %convert_element_type.82, () %tuple.61, (s32[]{:T(128)}, s32[128]{0:T(128)S(1)}, s32[]{:T(128)}, s32[128]{0:T(128)S(1)}, bf16[4,128,4,64]{1,3,2,0:T(8,128)(2,1)S(1)}, /*index=5*/s32[]{:T(128)}, bf16[128,4,64]{0,2,1:T(8,128)(2,1)S(1)}, ...), branch_computations={%region_2.2_spmd, %region_3.4_spmd} | conditional | flops 119505664 | bytes 1179684 | solution.py:76
  53.6 1.0 %fusion.11 = (f32[4,128]{1,0:T(4,128)}, f32[4,128,128]{1,2,0:T(8,128)S(1)}) fusion(pred[128,128]{0,1:T(8,128)(4,1)S(1)} %broadcast_compare_fusion, f32[4,128]{1,0:T(4,128)S(1)} %convert_bitcast_fusion, bf16[128,4,64]{0,2,1:T(8,128)(2,1)S(1)} %get-tuple-element.246, bf16[4,128,4,64]{1,3,2,0:T(8,128)(2,1)S(1)} %get-tuple-element.244, s32[]{:T(128)} %get-tuple-element.245), kind=kOutput, calls=%fused_computation.14 | convolution fusion | flops 9108992 | bytes 413700 | tf_op jit(solution)/shard_map/while/body/eval_jaxpr/cond/branch_1_fun/qhd,khd->hqk/dot_general | solution.py:15
  54.6 0.7 broadcast_multiply_fusion
  55.3 0.6 fusion.7
  55.9 0.2 fusion.14
  56.1 0.7 dynamic_update_slice.22
  56.8 0.6 dynamic_slice.50
  58.1 2.6 %conditional.3 = (f32[1,128,256]{1,2,0:T(8,128)S(1)}, f32[1,4,128]{2,1,0:T(4,128)}) conditional(s32[]{:T(128)} %convert_element_type.82, () %tuple.61, (s32[]{:T(128)}, s32[128]{0:T(128)S(1)}, s32[]{:T(128)}, s32[128]{0:T(128)S(1)}, bf16[4,128,4,64]{1,3,2,0:T(8,128)(2,1)S(1)}, /*index=5*/s32[]{:T(128)}, bf16[128,4,64]{0,2,1:T(8,128)(2,1)S(1)}, ...), branch_computations={%region_2.2_spmd, %region_3.4_spmd} | conditional | flops 119505664 | bytes 1179684 | solution.py:76
  58.2 1.0 %fusion.11 = (f32[4,128]{1,0:T(4,128)}, f32[4,128,128]{1,2,0:T(8,128)S(1)}) fusion(pred[128,128]{0,1:T(8,128)(4,1)S(1)} %broadcast_compare_fusion, f32[4,128]{1,0:T(4,128)S(1)} %convert_bitcast_fusion, bf16[128,4,64]{0,2,1:T(8,128)(2,1)S(1)} %get-tuple-element.246, bf16[4,128,4,64]{1,3,2,0:T(8,128)(2,1)S(1)} %get-tuple-element.244, s32[]{:T(128)} %get-tuple-element.245), kind=kOutput, calls=%fused_computation.14 | convolution fusion | flops 9108992 | bytes 413700 | tf_op jit(solution)/shard_map/while/body/eval_jaxpr/cond/branch_1_fun/qhd,khd->hqk/dot_general | solution.py:15
  59.2 0.7 broadcast_multiply_fusion
  59.9 0.6 fusion.7
  60.5 0.2 fusion.14
  60.7 0.7 dynamic_update_slice.22
  61.4 0.1 fusion.24
  61.6 0.1 copy.43
  61.7 13.7 %all_to_all.16 = bf16[4,32,256]{2,1,0:T(8,128)(2,1)S(1)} all-to-all(bf16[4,32,256]{2,1,0:T(8,128)(2,1)S(1)} %bitcast.54), channel_id=1, replica_groups=mesh['grp'=2,'sp'=4,'tp'=4] {'tp'}, dimensions={0} | all-to-all | bytes 131072 | tf_op jit(solution)/shard_map/all_to_all | solution.py:118
  75.4 3.0 %convolution_convert_fusion = bf16[32,2048]{1,0:T(8,128)(2,1)S(1)} fusion(bf16[32,1024]{1,0:T(8,128)(2,1)S(1)} %bitcast.53, bf16[1024,2048]{1,0:T(8,128)(2,1)} %all-gather.2.cloned.1.call-done), kind=kOutput, calls=%fused_computation.32 | convolution fusion | flops 134283264 | bytes 4390912 | tf_op jit(solution)/shard_map/dot_general | solution.py:120
  78.4 7.3 %all_gather.19 = bf16[128,2048]{1,0:T(8,128)(2,1)S(1)} all-gather(bf16[32,2048]{1,0:T(8,128)(2,1)S(1)} %convolution_convert_fusion), channel_id=1, replica_groups=mesh['grp'=2,'sp'=4,'tp'=4] {'tp'}, dimensions={0}, use_global_device_ids=true | all-gather | bytes 655360 | tf_op jit(solution)/shard_map/all_gather | solution.py:121
  85.7 0.8 copy.73
  (37 shorter events, 0.6 us)
Async XLA Ops:
  6.5 2.0 %copy-start = (bf16[2048,256]{1,0:T(8,128)(2,1)S(1)}, bf16[2048,256]{1,0:T(8,128)(2,1)}, u32[]{:S(2)}) copy-start(bf16[2048,256]{1,0:T(8,128)(2,1)} %param.14) | copy-start | bytes 3145732
  6.5 14.9 %copy-start.1 = (bf16[128,2048]{1,0:T(8,128)(2,1)S(1)}, bf16[128,2048]{1,0:T(8,128)(2,1)}, u32[]{:S(2)}) copy-start(bf16[128,2048]{1,0:T(8,128)(2,1)} %param.11) | copy-start | bytes 1572868
  6.5 14.9 %copy-start.3 = (f32[2048]{0:T(1024)S(1)}, f32[2048]{0:T(1024)}, u32[]{:S(2)}) copy-start(f32[2048]{0:T(1024)} %param.12) | copy-start | bytes 24580
  6.5 68.8 %all-gather.2.cloned.1.call-start = ((), (), s32[]{:S(2)}) async-start(), calls=%async_computation.1 | async-start | bytes 5242880 | tf_op jit(solution)/shard_map/all_gather | solution.py:119
  9.9 27.4 %copy-start.2 = (bf16[4,128]{1,0:T(4,128)(2,1)S(1)}, bf16[4,128]{1,0:T(4,128)(2,1)}, u32[]{:S(2)}) copy-start(bf16[4,128]{1,0:T(4,128)(2,1)} %param.17) | copy-start | bytes 3076
Sparse Core Ops, SparseCore 0:
  8.9 35.8 all-gather.1
where the time goes:
time: 93.8 us; the launch traced here: 93.3 us
  blocking collectives  49.5 us (53%)
  matrix products  14.6 us (16%)
  between operations  13.5 us (14%)
  local copies, waits for them, and re-layouts  7.46 us (8%)
  other arithmetic  4.42 us (5%)
  loops' own time  3.02 us (3%)
    all_to_all x1, blocking collectives, on_device(): lax.all_to_all(mixed, 'tp', split_axis=0, concat_axis=1, tiled=True)  13.7 us
    all_gather x1, blocking collectives, on_device(): piece_values = lax.all_gather(value_rows, 'sp', axis=0, tiled=True)  12 us
    all_gather x1, blocking collectives, on_device(): piece_keys = lax.all_gather(key_rows, 'sp', axis=0, tiled=True)  11 us
    all_gather x1, blocking collectives, on_device(): return lax.all_gather(own_rows, 'tp', axis=0, tiled=True)  7.28 us
    all_gather x1, blocking collectives, on_device(): piece_rates = lax.all_gather(rate_row_values, 'sp', axis=0, tiled=True)  5.6 us
    dot_general x4, matrix products, break_scores(): jnp.einsum('qhd,khd->hqk', query_heads, key_heads, preferred_element_type...  3.93 us
    dot_general x1, matrix products, on_device(): jnp.dot(token_heads, whole_out, preferred_element_type=F32).astype(BF16)  3.01 us
    dynamic_update_slice x4, local copies, waits for them, and re-layouts, absorb_one(): lax.dynamic_update_index_in_dim(inner_pair[1], remain, shard_index, 0)  2.88 us
  transfers between devices with their start and end apart: 1, of which 0 were waited for; matrix products, arithmetic and copies ran while one was open for 24% of the time, Pallas kernels for 0%

commit v1 on v0

--- a/solution.py
+++ b/solution.py
@@ -90,7 +90,12 @@
     )
     piece_keys = lax.all_gather(key_rows, "sp", axis=0, tiled=True)
     piece_values = lax.all_gather(value_rows, "sp", axis=0, tiled=True)
-    piece_rates = lax.all_gather(rate_row_values, "sp", axis=0, tiled=True)
+    ring = [rate_row_values]
+    for hop in range(3):
+        ring.append(lax.ppermute(ring[-1], "sp", [(dev, (dev + 1) % 4) for dev in range(4)]))
+    piece_rates = jnp.roll(
+        jnp.concatenate(ring[::-1], axis=0), (lax.axis_index("sp") + 1) * ring[0].shape[0], axis=0
+    )
     piece_count = piece_keys.shape[0] // row_count
     key_blocks = piece_keys.reshape(piece_count, row_count, heads_local, HD)
     value_blocks = piece_values.reshape(piece_count, row_count, heads_local, HD)

time: 93.8 us -> 89.4 us (0.953)
  blocking collectives: 49.5 us -> 42.9 us
  waiting for transfers between devices: 0.71 us -> 2.35 us
  starting transfers between devices: 0.01 us -> 1.56 us
  matrix products: 14.6 us -> 13.6 us
    all_gather x1 -> x0, blocking collectives: 5.6 us -> none  [on_device(): piece_rates = lax.all_gather(rate_row_values, 'sp', axis=0, tiled=True)]
    ppermute x0 -> x3, waiting for transfers between devices: none -> 1.67 us  [on_device(): lax.ppermute(ring[-1], 'sp', [(dev, (dev + 1) % 4) for dev in range(4)])]
    ppermute x0 -> x3, starting transfers between devices: none -> 1.53 us  [on_device(): lax.ppermute(ring[-1], 'sp', [(dev, (dev + 1) % 4) for dev in range(4)])]
    all_to_all x1, blocking collectives: 13.7 us -> 12.2 us  [on_device(): lax.all_to_all(mixed, 'tp', split_axis=0, concat_axis=1, tiled=True)]
    dot_general x1, matrix products: 1.58 us -> 0.37 us  [on_device(): queries = jnp.dot(normed, w_query, preferred_element_type=F32).astype(BF16)]
  transfers between devices with their start and end apart: 1 -> 4, of which waited for: 0 -> 1; matrix products, arithmetic and copies ran while one was open for 24% -> 24% of each run, Pallas kernels for 0% -> 0%
where the time goes in v1:
time: 89.4 us; the launch traced here: 88.9 us
  blocking collectives  42.9 us (48%)
  matrix products  13.6 us (15%)
  between operations  13.6 us (15%)
  local copies, waits for them, and re-layouts  7.51 us (8%)
  other arithmetic  4.41 us (5%)
  loops' own time  3.02 us (3%)
  waiting for transfers between devices  2.35 us (3%)
  starting transfers between devices  1.56 us (2%)
    all_gather x1, blocking collectives, on_device(): piece_values = lax.all_gather(value_rows, 'sp', axis=0, tiled=True)  12.3 us
    all_to_all x1, blocking collectives, on_device(): lax.all_to_all(mixed, 'tp', split_axis=0, concat_axis=1, tiled=True)  12.2 us
    all_gather x1, blocking collectives, on_device(): piece_keys = lax.all_gather(key_rows, 'sp', axis=0, tiled=True)  11.1 us
    all_gather x1, blocking collectives, on_device(): return lax.all_gather(own_rows, 'tp', axis=0, tiled=True)  7.28 us
    dot_general x4, matrix products, break_scores(): jnp.einsum('qhd,khd->hqk', query_heads, key_heads, preferred_element_type...  3.93 us
    dot_general x1, matrix products, on_device(): jnp.dot(token_heads, whole_out, preferred_element_type=F32).astype(BF16)  3.01 us
    dynamic_update_slice x4, local copies, waits for them, and re-layouts, absorb_one(): lax.dynamic_update_index_in_dim(inner_pair[1], remain, shard_index, 0)  2.88 us
    another operation x1, loops' own time, on_device(): lax.scan(absorb_one, initial, (jnp.arange(piece_count, dtype=jnp.int32),...  2.84 us
  transfers between devices with their start and end apart: 4, of which 1 were waited for; matrix products, arithmetic and copies ran while one was open for 24% of the time, Pallas kernels for 0%

profile of v1, /device:TPU:25, one launch (start us, length us, event | category | flops | bytes accessed | tf_op | source)
XLA Modules:
  0.0 88.9 jit_solution(10929664528696849787)
XLA Ops:
  6.6 0.7 all-gather.2.cloned.1.call-update
  7.3 1.2 %fusion.25 = f32[128]{0:T(128)S(1)} fusion(bf16[128,2048]{1,0:T(8,128)(2,1)} %param.11), kind=kLoop, calls=%fused_computation.40 | loop fusion | flops 786304 | bytes 524800 | tf_op jit(solution)/shard_map/reduce_sum | solution.py:49
  8.6 1.4 %convolution_convert_fusion.3 = bf16[128,256]{1,0:T(8,128)(2,1)S(1)} fusion(bf16[2048,256]{1,0:T(8,128)(2,1)S(1)} %copy-done, bf16[128,2048]{1,0:T(8,128)(2,1)} %param.11, f32[2048]{0:T(1024)} %param.12, f32[128]{0:T(128)S(1)} %add_rsqrt_fusion), kind=kOutput, calls=%fused_computation.37 | convolution fusion | flops 135299072 | bytes 1647104 | tf_op jit(solution)/shard_map/dot_general | solution.py:53
  10.0 1.8 %convolution_convert_fusion.1 = bf16[128,256]{1,0:T(8,128)(2,1)S(1)} fusion(bf16[2048,256]{1,0:T(8,128)(2,1)} %param.15, bf16[128,2048]{1,0:T(8,128)(2,1)} %param.11, f32[2048]{0:T(1024)} %param.12, f32[128]{0:T(128)S(1)} %add_rsqrt_fusion), kind=kOutput, calls=%fused_computation.35 | convolution fusion | flops 135299072 | bytes 1647104 | tf_op jit(solution)/shard_map/dot_general | solution.py:54
  11.8 0.4 convolution_convert_fusion.2
  12.2 11.1 %all_gather.12 = bf16[512,256]{1,0:T(8,128)(2,1)S(1)} all-gather(bf16[128,256]{1,0:T(8,128)(2,1)S(1)} %convolution_convert_fusion.3), channel_id=1, replica_groups=mesh['grp'=2,'sp'=4,'tp'=4] {'sp'}, dimensions={0}, use_global_device_ids=true | all-gather | bytes 327680 | tf_op jit(solution)/shard_map/all_gather | solution.py:91
  23.3 1.5 %collective-permute-start.1 = (bf16[128,4]{0,1:T(4,128)(2,1)S(1)}, bf16[128,4]{0,1:T(4,128)(2,1)S(1)}, u32[]{:S(2)}, u32[]{:S(2)}) collective-permute-start(bf16[128,4]{0,1:T(4,128)(2,1)S(1)} %collective-permute-done), channel_id=1, source_target_pairs={{0,4},{4,8},{8,12},{12,0},{1,5},{5,9},{9,13},{13,1},{2,6},{6,10},{... | collective-permute-start | bytes 3080 | tf_op jit(solution)/shard_map/ppermute | solution.py:95
  24.8 12.3 %all_gather.13 = bf16[512,256]{1,0:T(8,128)(2,1)S(1)} all-gather(bf16[128,256]{1,0:T(8,128)(2,1)S(1)} %convolution_convert_fusion.1), channel_id=1, replica_groups=mesh['grp'=2,'sp'=4,'tp'=4] {'sp'}, dimensions={0}, use_global_device_ids=true | all-gather | bytes 327680 | tf_op jit(solution)/shard_map/all_gather | solution.py:92
  37.1 0.2 reshape.91
  37.3 0.3 copy.39
  37.6 0.2 reshape.92
  37.9 0.3 copy.40
  38.1 0.1 copy.37
  38.3 1.7 %collective-permute-done.2 = bf16[128,4]{0,1:T(4,128)(2,1)S(1)} collective-permute-done((bf16[128,4]{0,1:T(4,128)(2,1)S(1)}, bf16[128,4]{0,1:T(4,128)(2,1)S(1)}, u32[]{:S(2)}, u32[]{:S(2)}) %collective-permute-start.2) | collective-permute-done | bytes 1056 | tf_op jit(solution)/shard_map/ppermute | solution.py:95
  40.1 18.4 %while.16 = (s32[]{:T(128)}, f32[4,128,256]{1,2,0:T(8,128)S(1)}, f32[4,4,128]{2,0,1:T(4,128)S(1)}, s32[4]{0:T(128)S(1)}, s32[]{:T(128)}, /*index=5*/s32[]{:T(128...) while((s32[]{:T(128)}, f32[4,128,256]{1,2,0:T(8,128)S(1)}, ...), condition=%wide.region_5.6_spmd.clone, body=%wide.region_1.5_spmd.clone.sunk | while | flops 119505664 | bytes 1446895 | solution.py:113
  40.1 0.6 dynamic_slice.56
  41.4 2.6 %conditional.3 = (f32[1,128,256]{1,2,0:T(8,128)S(1)}, f32[1,4,128]{2,1,0:T(4,128)}) conditional(s32[]{:T(128)} %convert_element_type.82, () %tuple.61, (s32[]{:T(128)}, s32[128]{0:T(128)S(1)}, s32[]{:T(128)}, s32[128]{0:T(128)S(1)}, bf16[4,128,4,64]{1,3,2,0:T(8,128)(2,1)S(1)}, /*index=5*/s32[]{:T(128)}, bf16[128,4,64]{0,2,1:T(8,128)(2,1)S(1)}, ...), branch_computations={%region_2.2_spmd, %region_3.4_spmd} | conditional | flops 119505664 | bytes 1179684 | solution.py:76
  41.5 1.0 %fusion.11 = (f32[4,128]{1,0:T(4,128)}, f32[4,128,128]{1,2,0:T(8,128)S(1)}) fusion(pred[128,128]{0,1:T(8,128)(4,1)S(1)} %broadcast_compare_fusion, f32[4,128]{1,0:T(4,128)S(1)} %convert_bitcast_fusion, bf16[128,4,64]{0,2,1:T(8,128)(2,1)S(1)} %get-tuple-element.246, bf16[4,128,4,64]{1,3,2,0:T(8,128)(2,1)S(1)} %get-tuple-element.244, s32[]{:T(128)} %get-tuple-element.245), kind=kOutput, calls=%fused_computation.14 | convolution fusion | flops 9108992 | bytes 413700 | tf_op jit(solution)/shard_map/while/body/eval_jaxpr/cond/branch_1_fun/qhd,khd->hqk/dot_general | solution.py:15
  42.5 0.7 broadcast_multiply_fusion
  43.2 0.6 fusion.7
  43.8 0.2 fusion.14
  44.0 0.7 dynamic_update_slice.22
  44.7 0.6 dynamic_slice.56
  46.0 2.6 %conditional.3 = (f32[1,128,256]{1,2,0:T(8,128)S(1)}, f32[1,4,128]{2,1,0:T(4,128)}) conditional(s32[]{:T(128)} %convert_element_type.82, () %tuple.61, (s32[]{:T(128)}, s32[128]{0:T(128)S(1)}, s32[]{:T(128)}, s32[128]{0:T(128)S(1)}, bf16[4,128,4,64]{1,3,2,0:T(8,128)(2,1)S(1)}, /*index=5*/s32[]{:T(128)}, bf16[128,4,64]{0,2,1:T(8,128)(2,1)S(1)}, ...), branch_computations={%region_2.2_spmd, %region_3.4_spmd} | conditional | flops 119505664 | bytes 1179684 | solution.py:76
  46.1 1.0 %fusion.11 = (f32[4,128]{1,0:T(4,128)}, f32[4,128,128]{1,2,0:T(8,128)S(1)}) fusion(pred[128,128]{0,1:T(8,128)(4,1)S(1)} %broadcast_compare_fusion, f32[4,128]{1,0:T(4,128)S(1)} %convert_bitcast_fusion, bf16[128,4,64]{0,2,1:T(8,128)(2,1)S(1)} %get-tuple-element.246, bf16[4,128,4,64]{1,3,2,0:T(8,128)(2,1)S(1)} %get-tuple-element.244, s32[]{:T(128)} %get-tuple-element.245), kind=kOutput, calls=%fused_computation.14 | convolution fusion | flops 9108992 | bytes 413700 | tf_op jit(solution)/shard_map/while/body/eval_jaxpr/cond/branch_1_fun/qhd,khd->hqk/dot_general | solution.py:15
  47.1 0.7 broadcast_multiply_fusion
  47.8 0.6 fusion.7
  48.4 0.2 fusion.14
  48.6 0.7 dynamic_update_slice.22
  49.3 0.6 dynamic_slice.56
  50.6 2.6 %conditional.3 = (f32[1,128,256]{1,2,0:T(8,128)S(1)}, f32[1,4,128]{2,1,0:T(4,128)}) conditional(s32[]{:T(128)} %convert_element_type.82, () %tuple.61, (s32[]{:T(128)}, s32[128]{0:T(128)S(1)}, s32[]{:T(128)}, s32[128]{0:T(128)S(1)}, bf16[4,128,4,64]{1,3,2,0:T(8,128)(2,1)S(1)}, /*index=5*/s32[]{:T(128)}, bf16[128,4,64]{0,2,1:T(8,128)(2,1)S(1)}, ...), branch_computations={%region_2.2_spmd, %region_3.4_spmd} | conditional | flops 119505664 | bytes 1179684 | solution.py:76
  50.7 1.0 %fusion.11 = (f32[4,128]{1,0:T(4,128)}, f32[4,128,128]{1,2,0:T(8,128)S(1)}) fusion(pred[128,128]{0,1:T(8,128)(4,1)S(1)} %broadcast_compare_fusion, f32[4,128]{1,0:T(4,128)S(1)} %convert_bitcast_fusion, bf16[128,4,64]{0,2,1:T(8,128)(2,1)S(1)} %get-tuple-element.246, bf16[4,128,4,64]{1,3,2,0:T(8,128)(2,1)S(1)} %get-tuple-element.244, s32[]{:T(128)} %get-tuple-element.245), kind=kOutput, calls=%fused_computation.14 | convolution fusion | flops 9108992 | bytes 413700 | tf_op jit(solution)/shard_map/while/body/eval_jaxpr/cond/branch_1_fun/qhd,khd->hqk/dot_general | solution.py:15
  51.7 0.7 broadcast_multiply_fusion
  52.4 0.6 fusion.7
  53.0 0.2 fusion.14
  53.2 0.7 dynamic_update_slice.22
  53.9 0.6 dynamic_slice.56
  55.2 2.6 %conditional.3 = (f32[1,128,256]{1,2,0:T(8,128)S(1)}, f32[1,4,128]{2,1,0:T(4,128)}) conditional(s32[]{:T(128)} %convert_element_type.82, () %tuple.61, (s32[]{:T(128)}, s32[128]{0:T(128)S(1)}, s32[]{:T(128)}, s32[128]{0:T(128)S(1)}, bf16[4,128,4,64]{1,3,2,0:T(8,128)(2,1)S(1)}, /*index=5*/s32[]{:T(128)}, bf16[128,4,64]{0,2,1:T(8,128)(2,1)S(1)}, ...), branch_computations={%region_2.2_spmd, %region_3.4_spmd} | conditional | flops 119505664 | bytes 1179684 | solution.py:76
  55.3 1.0 %fusion.11 = (f32[4,128]{1,0:T(4,128)}, f32[4,128,128]{1,2,0:T(8,128)S(1)}) fusion(pred[128,128]{0,1:T(8,128)(4,1)S(1)} %broadcast_compare_fusion, f32[4,128]{1,0:T(4,128)S(1)} %convert_bitcast_fusion, bf16[128,4,64]{0,2,1:T(8,128)(2,1)S(1)} %get-tuple-element.246, bf16[4,128,4,64]{1,3,2,0:T(8,128)(2,1)S(1)} %get-tuple-element.244, s32[]{:T(128)} %get-tuple-element.245), kind=kOutput, calls=%fused_computation.14 | convolution fusion | flops 9108992 | bytes 413700 | tf_op jit(solution)/shard_map/while/body/eval_jaxpr/cond/branch_1_fun/qhd,khd->hqk/dot_general | solution.py:15
  56.3 0.7 broadcast_multiply_fusion
  57.0 0.6 fusion.7
  57.6 0.2 fusion.14
  57.8 0.7 dynamic_update_slice.22
  58.5 0.1 fusion.24
  58.8 12.2 %all_to_all.16 = bf16[4,32,256]{2,1,0:T(8,128)(2,1)S(1)} all-to-all(bf16[4,32,256]{2,1,0:T(8,128)(2,1)S(1)} %bitcast.57), channel_id=1, replica_groups=mesh['grp'=2,'sp'=4,'tp'=4] {'tp'}, dimensions={0} | all-to-all | bytes 131072 | tf_op jit(solution)/shard_map/all_to_all | solution.py:123
  71.0 3.0 %convolution_convert_fusion = bf16[32,2048]{1,0:T(8,128)(2,1)S(1)} fusion(bf16[32,1024]{1,0:T(8,128)(2,1)S(1)} %bitcast.56, bf16[1024,2048]{1,0:T(8,128)(2,1)} %all-gather.2.cloned.1.call-done), kind=kOutput, calls=%fused_computation.32 | convolution fusion | flops 134283264 | bytes 4390912 | tf_op jit(solution)/shard_map/dot_general | solution.py:125
  74.0 7.3 %all_gather.15 = bf16[128,2048]{1,0:T(8,128)(2,1)S(1)} all-gather(bf16[32,2048]{1,0:T(8,128)(2,1)S(1)} %convolution_convert_fusion), channel_id=1, replica_groups=mesh['grp'=2,'sp'=4,'tp'=4] {'tp'}, dimensions={0}, use_global_device_ids=true | all-gather | bytes 655360 | tf_op jit(solution)/shard_map/all_gather | solution.py:126
  81.3 0.8 copy.80
  (53 shorter events, 0.9 us)
Async XLA Ops:
  6.5 2.0 %copy-start = (bf16[2048,256]{1,0:T(8,128)(2,1)S(1)}, bf16[2048,256]{1,0:T(8,128)(2,1)}, u32[]{:S(2)}) copy-start(bf16[2048,256]{1,0:T(8,128)(2,1)} %param.14) | copy-start | bytes 3145732
  6.5 5.2 %copy-start.1 = (bf16[128,2048]{1,0:T(8,128)(2,1)S(1)}, bf16[128,2048]{1,0:T(8,128)(2,1)}, u32[]{:S(2)}) copy-start(bf16[128,2048]{1,0:T(8,128)(2,1)} %param.11) | copy-start | bytes 1572868
  6.5 5.2 %copy-start.4 = (f32[2048]{0:T(1024)S(1)}, f32[2048]{0:T(1024)}, u32[]{:S(2)}) copy-start(f32[2048]{0:T(1024)} %param.12) | copy-start | bytes 24580
  6.5 5.3 %copy-start.3 = (bf16[2048,256]{1,0:T(8,128)(2,1)S(1)}, bf16[2048,256]{1,0:T(8,128)(2,1)}, u32[]{:S(2)}) copy-start(bf16[2048,256]{1,0:T(8,128)(2,1)} %param.13) | copy-start | bytes 3145732
  6.5 64.5 %all-gather.2.cloned.1.call-start = ((), (), s32[]{:S(2)}) async-start(), calls=%async_computation.1 | async-start | bytes 5242880 | tf_op jit(solution)/shard_map/all_gather | solution.py:124
  7.3 16.0 %collective-permute-start = (bf16[128,4]{0,1:T(4,128)(2,1)}, bf16[128,4]{0,1:T(4,128)(2,1)S(1)}, u32[]{:S(2)}, u32[]{:S(2)}) collective-permute-start(bf16[128,4]{0,1:T(4,128)(2,1)} %bitcast.60), channel_id=1, source_target_pairs={{0,4},{4,8},{8,12},{12,0},{1,5},{5,9},{9,13},{13,1},{2,6},{6,10},{... | collective-permute-start | bytes 3080 | tf_op jit(solution)/shard_map/ppermute | solution.py:95
  10.0 29.9 %copy-start.2 = (bf16[4,128]{1,0:T(4,128)(2,1)S(1)}, bf16[4,128]{1,0:T(4,128)(2,1)}, u32[]{:S(2)}) copy-start(bf16[4,128]{1,0:T(4,128)(2,1)} %param.17) | copy-start | bytes 3076
  23.3 13.8 %collective-permute-start.1 = (bf16[128,4]{0,1:T(4,128)(2,1)S(1)}, bf16[128,4]{0,1:T(4,128)(2,1)S(1)}, u32[]{:S(2)}, u32[]{:S(2)}) collective-permute-start(bf16[128,4]{0,1:T(4,128)(2,1)S(1)} %collective-permute-done), channel_id=1, source_target_pairs={{0,4},{4,8},{8,12},{12,0},{1,5},{5,9},{9,13},{13,1},{2,6},{6,10},{... | collective-permute-start | bytes 3080 | tf_op jit(solution)/shard_map/ppermute | solution.py:95
  37.1 2.8 %collective-permute-start.2 = (bf16[128,4]{0,1:T(4,128)(2,1)S(1)}, bf16[128,4]{0,1:T(4,128)(2,1)S(1)}, u32[]{:S(2)}, u32[]{:S(2)}) collective-permute-start(bf16[128,4]{0,1:T(4,128)(2,1)S(1)} %collective-permute-done.1), channel_id=1, source_target_pairs={{0,4},{4,8},{8,12},{12,0},{1,5},{5,9},{9,13},{13,1},{2,6},{6,10},{... | collective-permute-start | bytes 3080 | tf_op jit(solution)/shard_map/ppermute | solution.py:95
Sparse Core Ops, SparseCore 0:
  8.9 35.8 all-gather.1
